TPU v7x, 32 devices: a whole 2x2x4 slice. The times are simulated.
32 devices in a mesh: sp: 8 (over z, x), tp: 4 (over y, core).
Axes of the slice: x: 2, y: 2, z: 4, core: 2. Of those that a mesh axis runs over, the one named last changes fastest.
Arguments:
- query_main: bfloat16 [1024, 2048], P('sp', 'tp'), may hold values from -6 to 6
- query_rotary: bfloat16 [1024, 1024], P('sp', 'tp'), may hold values from -7 to 7
- latent: bfloat16 [1024, 512], P('sp'), may hold values from -8 to 8
- key_rotary: bfloat16 [1024, 64], P('sp'), may hold values from -8 to 8
- key_weight: bfloat16 [512, 2048], P(None, 'tp'), may hold values from -0.25 to 0.25
- value_weight: bfloat16 [512, 2048], P(None, 'tp'), may hold values from -0.25 to 0.25
- head_output: bfloat16 [1024, 2048], P('sp', 'tp'), may hold values from -2 to 2
- output_grad: bfloat16 [1024, 2048], P('sp', 'tp'), may hold values from -40 to 40
- row_logsum: float32 [16, 1024], P('tp', 'sp'), may hold values from 3 to 16, as said below
Outputs:
- grad_query_main: float32 [1024, 2048], P('sp', 'tp')
- grad_query_rotary: float32 [1024, 1024], P('sp', 'tp')
- grad_latent: float32 [1024, 512], P('sp')
- grad_key_rotary: float32 [1024, 64], P('sp')
- grad_key_weight: float32 [512, 2048], P('sp', 'tp')
Inputs may be any that keep to these rules, and one draw needn't show every extreme that they name: With p the place of token i in its sequence and q = i % 128, row_logsum[h, i] minus the logarithm of (p + 1 + 54 (q + 1)) lies between -0.3 and 1.5.
All inputs are finite; a program needn't handle non-finite values.
Results may differ from a plain program's by a relative error of at most 0.003.
The roundings to bfloat16 on the way count: a program that leaves them out, or rounds other values in their place, can miss the bound.
Values may be sent and summed in bfloat16 or wider, within the bound.
A program may use at most 64 MiB of HBM per device.

v0:
```python
import jax
import jax.numpy as jnp
from jax import lax
from jax.sharding import PartitionSpec as P

SEQ_DEVICES = 32


def shifted(shard, axis, by):
    peers = lax.axis_size(axis)
    pairs = [(i, i + by) for i in range(peers) if 0 <= i + by < peers]
    return lax.ppermute(shard, axis, pairs)


def from_behind(block, axis, distance):
    devices = range(lax.axis_size(axis))
    route = [((i - distance) % len(devices), i) for i in devices]
    return lax.ppermute(block, axis, route)


def per_device(
    query_main,
    query_rotary,
    latent,
    key_rotary,
    key_weight,
    value_weight,
    head_output,
    output_grad,
    row_logsum,
):
    devices = lax.axis_size("sp")
    my_index = lax.axis_index("sp")
    group_span = min(SEQ_DEVICES, devices)
    lead_span = group_span // 4
    own_sequence = (my_index + lead_span) // group_span
    heads_here, tok_rows = row_logsum.shape
    lat_width = latent.shape[1]
    rot_width = key_rotary.shape[1]
    main_width = key_weight.shape[1] // heads_here
    value_width = value_weight.shape[1] // heads_here
    factor = (main_width + rot_width) ** (-0.5)
    main_query = query_main.reshape(tok_rows, heads_here, main_width)
    rot_query = query_rotary.reshape(tok_rows, heads_here, rot_width)
    key_proj = key_weight.reshape(lat_width, heads_here, main_width)
    value_proj = value_weight.reshape(lat_width, heads_here, value_width)
    grad_heads = output_grad.reshape(tok_rows, heads_here, value_width)
    query_latent = jnp.einsum(
        "thd,lhd->thl", main_query, key_proj, preferred_element_type=jnp.float32
    ).astype(jnp.bfloat16)
    grad_rows = jnp.einsum(
        "thd,lhd->thl", grad_heads, value_proj, preferred_element_type=jnp.float32
    ).astype(jnp.bfloat16)
    row_terms = jnp.sum(
        head_output.reshape(tok_rows, heads_here, value_width).astype(jnp.float32)
        * grad_heads.astype(jnp.float32),
        axis=2,
    )
    row_logs = row_logsum.T
    query_place = my_index * tok_rows + jnp.arange(tok_rows)

    def attend_block(state, key_block, grad_block, block_index, first_row):
        mixed_sum, rot_sum = state
        lat_block, rot_block = key_block
        acc_lat, acc_rot = grad_block
        key_place = block_index * tok_rows + first_row + jnp.arange(lat_block.shape[0])
        seen = key_place[None, :] <= query_place[:, None]
        scores = jnp.einsum(
            "thl,kl->thk", query_latent, lat_block, preferred_element_type=jnp.float32
        )
        scores = scores + jnp.einsum(
            "thr,kr->thk", rot_query, rot_block, preferred_element_type=jnp.float32
        )
        weights = jnp.where(seen[:, None, :], jnp.exp(factor * scores - row_logs[:, :, None]), 0.0)
        slopes = jnp.einsum("thl,kl->thk", grad_rows, lat_block, preferred_element_type=jnp.float32)
        dscores = weights * (slopes - row_terms[:, :, None])
        weights_low = weights.astype(jnp.bfloat16)
        dscores_low = dscores.astype(jnp.bfloat16)
        mixed_sum = mixed_sum + jnp.einsum(
            "thk,kl->thl", dscores_low, lat_block, preferred_element_type=jnp.float32
        )
        rot_sum = rot_sum + jnp.einsum(
            "thk,kr->thr", dscores_low, rot_block, preferred_element_type=jnp.float32
        )
        part_lat = factor * jnp.einsum(
            "thk,thl->kl", dscores_low, query_latent, preferred_element_type=jnp.float32
        )
        part_lat = part_lat + jnp.einsum(
            "thk,thl->kl", weights_low, grad_rows, preferred_element_type=jnp.float32
        )
        part_rot = factor * jnp.einsum(
            "thk,thr->kr", dscores_low, rot_query, preferred_element_type=jnp.float32
        )
        return ((mixed_sum, rot_sum), (acc_lat + part_lat, acc_rot + part_rot))

    def visit_block(state, key_block, grad_block, block_index, first_row):
        useful = ((block_index + lead_span) // group_span == own_sequence) & (
            block_index <= my_index
        )

        def work(operand):
            return attend_block(operand[0], key_block, operand[1], block_index, first_row)

        def skip(operand):
            return operand

        return lax.cond(useful, work, skip, (state, grad_block))

    zero_state = (
        jnp.zeros((tok_rows, heads_here, lat_width), jnp.float32),
        jnp.zeros((tok_rows, heads_here, rot_width), jnp.float32),
    )
    zero_grads = (
        jnp.zeros((tok_rows, lat_width), jnp.float32),
        jnp.zeros((tok_rows, rot_width), jnp.float32),
    )

    def forward_step(step, carry):
        state, key_block, grad_block = carry
        state, grad_block = visit_block(
            state, key_block, grad_block, (my_index - step) % devices, 0
        )
        key_block = shifted((key_block[0], key_block[1]), "sp", 1)
        grad_block = from_behind((grad_block[0], grad_block[1]), "sp", 1)
        return (state, key_block, grad_block)

    state, key_block, grad_block = lax.fori_loop(
        0, group_span - 1, forward_step, (zero_state, (latent, key_rotary), zero_grads)
    )
    state, grad_block = visit_block(
        state, key_block, grad_block, (my_index + 1 - group_span) % devices, 0
    )
    lat_grad, rot_grad = from_behind((grad_block[0], grad_block[1]), "sp", 1 - group_span)
    lat_grad, rot_grad = lax.psum((lat_grad, rot_grad), "tp")
    mixed_sum, rot_sum = state
    mixed_low = mixed_sum.astype(jnp.bfloat16)
    grad_main = factor * jnp.einsum(
        "thl,lhd->thd", mixed_low, key_proj, preferred_element_type=jnp.float32
    )
    term = jnp.einsum("thl,thd->lhd", mixed_low, main_query, preferred_element_type=jnp.float32)
    grad_weight = lax.psum_scatter(
        factor
        * term.reshape(lax.axis_size("sp") * (lat_width // devices), heads_here * main_width),
        "sp",
        scatter_dimension=0,
        tiled=True,
    )
    return (
        grad_main.reshape(tok_rows, heads_here * main_width),
        (factor * rot_sum).reshape(tok_rows, heads_here * rot_width),
        lat_grad,
        rot_grad,
        grad_weight,
    )


def solution(mesh):
    return jax.shard_map(
        per_device,
        mesh=mesh,
        in_specs=(
            P("sp", "tp"),
            P("sp", "tp"),
            P("sp", None),
            P("sp", None),
            P(None, "tp"),
            P(None, "tp"),
            P("sp", "tp"),
            P("sp", "tp"),
            P("tp", "sp"),
        ),
        out_specs=(P("sp", "tp"), P("sp", "tp"), P("sp", None), P("sp", None), P("sp", "tp")),
        check_vma=False,
    )
```

profile of v0, /device:TPU:1, one launch (start us, length us, event | category | flops | bytes accessed | tf_op | source)
XLA Modules:
  0.0 204.9 jit_solution(4376401156759301379)
XLA Ops:
  8.1 1.3 copy.76
  11.9 0.8 copy-done.15
  13.1 0.8 copy-done.18
  15.6 95.9 %while.26 = (s32[]{:T(128)}, f32[128,4,512]{2,0,1:T(8,128)S(1)}, f32[128,4,64]{0,2,1:T(8,128)}, bf16[128,512]{1,0:T(8,128)(2,1)S(1)}, bf16[128,64]{0,1:T(8,128)(...) while((s32[]{:T(128)}, f32[128,4,512]{2,0,1:T(8,128)S(1)}, ...), condition=%wide.region_4.5_spmd.clone, body=%wide.region_1.4_spmd.clone.sunk | while | flops 361759008 | bytes 10788710 | solution.py:127
  15.7 3.7 %conditional.5 = ((f32[128,4,512]{2,0,1:T(8,128)S(1)}, f32[128,4,64]{0,2,1:T(8,128)}, f32[128,512]{1,0:T(8,128)S(1)}, f32[128,64]{0,1:T(8,128)S(1)})) conditional(s32[]{:T(128)} %convert_element_type.84, (f32[128,4,512]{2,0,1:T(8,128)S(1)}, f32[128,4,64]{0,2,1:T(8,128)}, f32[128,512]{1,0:T(8,128)S(1)}, f32[128,64]{0,1:T(8,128)S(1)}) %tuple.83, ...), branch_computations={%region_2.2_spmd, %region_3.3_spmd} | conditional | flops 361758976 | bytes 8133180 | solution.py:107
  17.5 1.7 convolution_add_fusion.2
  19.4 2.1 %collective-permute-start.2 = (f32[128,512]{1,0:T(8,128)S(1)}, f32[128,512]{1,0:T(8,128)S(1)}, u32[]{:S(2)}, u32[]{:S(2)}) collective-permute-start(f32[128,512]{1,0:T(8,128)S(1)} %get-tuple-element.773), channel_id=1, source_target_pairs={{28,0},{0,4},{4,8},{8,12},{12,16},{16,20},{20,24},{24,28},{29,1},{... | collective-permute-start | bytes 786440 | tf_op jit(solution)/shard_map/while/body/eval_jaxpr/ppermute | solution.py:18
  21.5 3.2 %collective-permute-start = (bf16[128,512]{1,0:T(8,128)(2,1)S(1)}, bf16[128,512]{1,0:T(8,128)(2,1)S(1)}, u32[]{:S(2)}, u32[]{:S(2)}) collective-permute-start(bf16[128,512]{1,0:T(8,128)(2,1)S(1)} %copy.106), channel_id=1, source_target_pairs={{0,4},{4,8},{8,12},{12,16},{16,20},{20,24},{24,28},{1,5},{5,9},{9,... | collective-permute-start | bytes 393224 | tf_op jit(solution)/shard_map/while/body/eval_jaxpr/ppermute | solution.py:12
  24.7 1.2 collective-permute-start.3
  26.0 3.2 %collective-permute-start.1 = (bf16[128,64]{0,1:T(8,128)(2,1)S(1)}, bf16[128,64]{0,1:T(8,128)(2,1)S(1)}, u32[]{:S(2)}, u32[]{:S(2)}) collective-permute-start(bf16[128,64]{0,1:T(8,128)(2,1)S(1)} %copy.107), channel_id=1, source_target_pairs={{0,4},{4,8},{8,12},{12,16},{16,20},{20,24},{24,28},{1,5},{5,9},{9,... | collective-permute-start | bytes 49160 | tf_op jit(solution)/shard_map/while/body/eval_jaxpr/ppermute | solution.py:12
  29.1 2.2 %collective-permute-done.3 = f32[128,64]{0,1:T(8,128)} collective-permute-done((f32[128,64]{0,1:T(8,128)S(1)}, f32[128,64]{0,1:T(8,128)}, u32[]{:S(2)}, u32[]{:S(2)}) %collective-permute-start.3) | collective-permute-done | bytes 32800 | tf_op jit(solution)/shard_map/while/body/eval_jaxpr/ppermute | solution.py:18
  31.3 0.8 copy.116
  32.2 4.7 %collective-permute-start.2 = (f32[128,512]{1,0:T(8,128)S(1)}, f32[128,512]{1,0:T(8,128)S(1)}, u32[]{:S(2)}, u32[]{:S(2)}) collective-permute-start(f32[128,512]{1,0:T(8,128)S(1)} %get-tuple-element.773), channel_id=1, source_target_pairs={{28,0},{0,4},{4,8},{8,12},{12,16},{16,20},{20,24},{24,28},{29,1},{... | collective-permute-start | bytes 786440 | tf_op jit(solution)/shard_map/while/body/eval_jaxpr/ppermute | solution.py:18
  36.9 4.1 %collective-permute-start = (bf16[128,512]{1,0:T(8,128)(2,1)S(1)}, bf16[128,512]{1,0:T(8,128)(2,1)S(1)}, u32[]{:S(2)}, u32[]{:S(2)}) collective-permute-start(bf16[128,512]{1,0:T(8,128)(2,1)S(1)} %copy.106), channel_id=1, source_target_pairs={{0,4},{4,8},{8,12},{12,16},{16,20},{20,24},{24,28},{1,5},{5,9},{9,... | collective-permute-start | bytes 393224 | tf_op jit(solution)/shard_map/while/body/eval_jaxpr/ppermute | solution.py:12
  41.3 4.1 %collective-permute-start.1 = (bf16[128,64]{0,1:T(8,128)(2,1)S(1)}, bf16[128,64]{0,1:T(8,128)(2,1)S(1)}, u32[]{:S(2)}, u32[]{:S(2)}) collective-permute-start(bf16[128,64]{0,1:T(8,128)(2,1)S(1)} %copy.107), channel_id=1, source_target_pairs={{0,4},{4,8},{8,12},{12,16},{16,20},{20,24},{24,28},{1,5},{5,9},{9,... | collective-permute-start | bytes 49160 | tf_op jit(solution)/shard_map/while/body/eval_jaxpr/ppermute | solution.py:12
  45.4 1.7 collective-permute-done.3
  47.2 0.8 copy.116
  48.6 7.5 %collective-permute-start = (bf16[128,512]{1,0:T(8,128)(2,1)S(1)}, bf16[128,512]{1,0:T(8,128)(2,1)S(1)}, u32[]{:S(2)}, u32[]{:S(2)}) collective-permute-start(bf16[128,512]{1,0:T(8,128)(2,1)S(1)} %copy.106), channel_id=1, source_target_pairs={{0,4},{4,8},{8,12},{12,16},{16,20},{20,24},{24,28},{1,5},{5,9},{9,... | collective-permute-start | bytes 393224 | tf_op jit(solution)/shard_map/while/body/eval_jaxpr/ppermute | solution.py:12
  56.3 4.2 %collective-permute-start.1 = (bf16[128,64]{0,1:T(8,128)(2,1)S(1)}, bf16[128,64]{0,1:T(8,128)(2,1)S(1)}, u32[]{:S(2)}, u32[]{:S(2)}) collective-permute-start(bf16[128,64]{0,1:T(8,128)(2,1)S(1)} %copy.107), channel_id=1, source_target_pairs={{0,4},{4,8},{8,12},{12,16},{16,20},{20,24},{24,28},{1,5},{5,9},{9,... | collective-permute-start | bytes 49160 | tf_op jit(solution)/shard_map/while/body/eval_jaxpr/ppermute | solution.py:12
  60.6 1.2 collective-permute-done.3
  62.7 1.0 collective-permute-start.2
  63.8 2.8 %collective-permute-start = (bf16[128,512]{1,0:T(8,128)(2,1)S(1)}, bf16[128,512]{1,0:T(8,128)(2,1)S(1)}, u32[]{:S(2)}, u32[]{:S(2)}) collective-permute-start(bf16[128,512]{1,0:T(8,128)(2,1)S(1)} %copy.106), channel_id=1, source_target_pairs={{0,4},{4,8},{8,12},{12,16},{16,20},{20,24},{24,28},{1,5},{5,9},{9,... | collective-permute-start | bytes 393224 | tf_op jit(solution)/shard_map/while/body/eval_jaxpr/ppermute | solution.py:12
  66.6 4.6 %collective-permute-start.3 = (f32[128,64]{0,1:T(8,128)S(1)}, f32[128,64]{0,1:T(8,128)}, u32[]{:S(2)}, u32[]{:S(2)}) collective-permute-start(f32[128,64]{0,1:T(8,128)S(1)} %get-tuple-element.774), channel_id=1, source_target_pairs={{28,0},{0,4},{4,8},{8,12},{12,16},{16,20},{20,24},{24,28},{29,1},{... | collective-permute-start | bytes 98312 | tf_op jit(solution)/shard_map/while/body/eval_jaxpr/ppermute | solution.py:18
  71.2 3.4 %collective-permute-start.1 = (bf16[128,64]{0,1:T(8,128)(2,1)S(1)}, bf16[128,64]{0,1:T(8,128)(2,1)S(1)}, u32[]{:S(2)}, u32[]{:S(2)}) collective-permute-start(bf16[128,64]{0,1:T(8,128)(2,1)S(1)} %copy.107), channel_id=1, source_target_pairs={{0,4},{4,8},{8,12},{12,16},{16,20},{20,24},{24,28},{1,5},{5,9},{9,... | collective-permute-start | bytes 49160 | tf_op jit(solution)/shard_map/while/body/eval_jaxpr/ppermute | solution.py:12
  74.6 0.8 copy.116
  75.6 1.8 collective-permute-start.2
  77.3 3.3 %collective-permute-start = (bf16[128,512]{1,0:T(8,128)(2,1)S(1)}, bf16[128,512]{1,0:T(8,128)(2,1)S(1)}, u32[]{:S(2)}, u32[]{:S(2)}) collective-permute-start(bf16[128,512]{1,0:T(8,128)(2,1)S(1)} %copy.106), channel_id=1, source_target_pairs={{0,4},{4,8},{8,12},{12,16},{16,20},{20,24},{24,28},{1,5},{5,9},{9,... | collective-permute-start | bytes 393224 | tf_op jit(solution)/shard_map/while/body/eval_jaxpr/ppermute | solution.py:12
  80.6 1.2 collective-permute-start.3
  81.8 5.5 %collective-permute-start.1 = (bf16[128,64]{0,1:T(8,128)(2,1)S(1)}, bf16[128,64]{0,1:T(8,128)(2,1)S(1)}, u32[]{:S(2)}, u32[]{:S(2)}) collective-permute-start(bf16[128,64]{0,1:T(8,128)(2,1)S(1)} %copy.107), channel_id=1, source_target_pairs={{0,4},{4,8},{8,12},{12,16},{16,20},{20,24},{24,28},{1,5},{5,9},{9,... | collective-permute-start | bytes 49160 | tf_op jit(solution)/shard_map/while/body/eval_jaxpr/ppermute | solution.py:12
  87.3 0.8 copy.116
  88.2 2.2 %collective-permute-start.2 = (f32[128,512]{1,0:T(8,128)S(1)}, f32[128,512]{1,0:T(8,128)S(1)}, u32[]{:S(2)}, u32[]{:S(2)}) collective-permute-start(f32[128,512]{1,0:T(8,128)S(1)} %get-tuple-element.773), channel_id=1, source_target_pairs={{28,0},{0,4},{4,8},{8,12},{12,16},{16,20},{20,24},{24,28},{29,1},{... | collective-permute-start | bytes 786440 | tf_op jit(solution)/shard_map/while/body/eval_jaxpr/ppermute | solution.py:18
  90.5 2.8 %collective-permute-start = (bf16[128,512]{1,0:T(8,128)(2,1)S(1)}, bf16[128,512]{1,0:T(8,128)(2,1)S(1)}, u32[]{:S(2)}, u32[]{:S(2)}) collective-permute-start(bf16[128,512]{1,0:T(8,128)(2,1)S(1)} %copy.106), channel_id=1, source_target_pairs={{0,4},{4,8},{8,12},{12,16},{16,20},{20,24},{24,28},{1,5},{5,9},{9,... | collective-permute-start | bytes 393224 | tf_op jit(solution)/shard_map/while/body/eval_jaxpr/ppermute | solution.py:12
  93.3 1.2 collective-permute-start.3
  94.5 1.9 collective-permute-start.1
  96.4 2.5 %collective-permute-done.3 = f32[128,64]{0,1:T(8,128)} collective-permute-done((f32[128,64]{0,1:T(8,128)S(1)}, f32[128,64]{0,1:T(8,128)}, u32[]{:S(2)}, u32[]{:S(2)}) %collective-permute-start.3) | collective-permute-done | bytes 32800 | tf_op jit(solution)/shard_map/while/body/eval_jaxpr/ppermute | solution.py:18
  100.1 5.0 %collective-permute-start = (bf16[128,512]{1,0:T(8,128)(2,1)S(1)}, bf16[128,512]{1,0:T(8,128)(2,1)S(1)}, u32[]{:S(2)}, u32[]{:S(2)}) collective-permute-start(bf16[128,512]{1,0:T(8,128)(2,1)S(1)} %copy.106), channel_id=1, source_target_pairs={{0,4},{4,8},{8,12},{12,16},{16,20},{20,24},{24,28},{1,5},{5,9},{9,... | collective-permute-start | bytes 393224 | tf_op jit(solution)/shard_map/while/body/eval_jaxpr/ppermute | solution.py:12
  105.2 2.0 collective-permute-start.1
  107.1 3.6 %collective-permute-done.3 = f32[128,64]{0,1:T(8,128)} collective-permute-done((f32[128,64]{0,1:T(8,128)S(1)}, f32[128,64]{0,1:T(8,128)}, u32[]{:S(2)}, u32[]{:S(2)}) %collective-permute-start.3) | collective-permute-done | bytes 32800 | tf_op jit(solution)/shard_map/while/body/eval_jaxpr/ppermute | solution.py:18
  111.6 8.4 %collective-permute-done.4 = f32[128,512]{1,0:T(8,128)S(1)} collective-permute-done((f32[128,512]{1,0:T(8,128)S(1)}, f32[128,512]{1,0:T(8,128)S(1)}, u32[]{:S(2)}, u32[]{:S(2)}) %collective-permute-start.4) | collective-permute-done | bytes 262176 | tf_op jit(solution)/shard_map/ppermute | solution.py:18
  121.3 1.3 copy.67
  122.8 0.9 copy-done.7
  124.0 0.9 broadcast_multiply_fusion
  125.0 0.8 copy.68
  126.5 2.3 %collective-permute-done.5 = f32[128,64]{0,1:T(8,128)S(1)} collective-permute-done((f32[128,64]{0,1:T(8,128)S(1)}, f32[128,64]{0,1:T(8,128)S(1)}, u32[]{:S(2)}, u32[]{:S(2)}) %collective-permute-start.5) | collective-permute-done | bytes 32800 | tf_op jit(solution)/shard_map/ppermute | solution.py:18
  128.9 22.4 %psum.15 = f32[128,64]{0,1:T(8,128)} all-reduce(f32[128,64]{0,1:T(8,128)S(1)} %collective-permute-done.5), channel_id=1, replica_groups=mesh['sp'=8,'tp'=4] {'tp'}, use_global_device_ids=true, to_apply=%region_8.9 | all-reduce | flops 8192 | bytes 65536 | tf_op jit(solution)/shard_map/psum | solution.py:134
  151.2 8.7 %all-reduce.2.cloned.1.call-done = f32[128,512]{1,0:T(8,128)} async-done(((f32[128,512]{1,0:T(8,128)}), f32[128,512]{1,0:T(8,128)}) %all-reduce.2.cloned.1.call-update) | async-done | bytes 262160 | tf_op jit(solution)/shard_map/psum | solution.py:134
  159.9 35.9 %reduce-scatter.2.cloned.1.call-done = f32[64,512]{1,0:T(8,128)} async-done(((f32[512,512]{1,0:T(8,128)}), f32[64,512]{1,0:T(8,128)}) %reduce-scatter.2.cloned.1.call-update) | async-done | bytes 131088 | tf_op jit(solution)/shard_map/reduce_scatter | solution.py:141
  195.8 1.7 copy.131
  (128 shorter events, 12.9 us)
Async XLA Ops:
  8.0 3.3 %copy-start = (bf16[512,512]{1,0:T(8,128)(2,1)S(1)}, bf16[512,512]{1,0:T(8,128)(2,1)}, u32[]{:S(2)}) copy-start(bf16[512,512]{1,0:T(8,128)(2,1)} %param.20) | copy-start | bytes 1572868
  8.0 151.9 %all-reduce.2.cloned.1.call-start = ((), (), s32[]{:S(2)}) async-start(), calls=%async_computation.1 | async-start | bytes 524288 | tf_op jit(solution)/shard_map/psum | solution.py:134
  8.1 1.3 copy-start.16
  9.4 0.8 copy-start.6
  9.6 0.7 copy-start.8
  10.3 0.8 copy-start.2
  10.3 1.0 copy-start.13
  11.6 1.1 copy-start.4
  11.7 1.0 copy-start.15
  13.0 1.0 copy-start.11
  13.0 0.9 copy-start.18
  14.2 1.0 copy-start.1
  14.9 0.7 copy-start.10
  14.9 0.7 copy-start.17
  19.4 12.6 %collective-permute-start.2 = (f32[128,512]{1,0:T(8,128)S(1)}, f32[128,512]{1,0:T(8,128)S(1)}, u32[]{:S(2)}, u32[]{:S(2)}) collective-permute-start(f32[128,512]{1,0:T(8,128)S(1)} %get-tuple-element.773), channel_id=1, source_target_pairs={{28,0},{0,4},{4,8},{8,12},{12,16},{16,20},{20,24},{24,28},{29,1},{... | collective-permute-start | bytes 786440 | tf_op jit(solution)/shard_map/while/body/eval_jaxpr/ppermute | solution.py:18
  21.5 10.6 %collective-permute-start = (bf16[128,512]{1,0:T(8,128)(2,1)S(1)}, bf16[128,512]{1,0:T(8,128)(2,1)S(1)}, u32[]{:S(2)}, u32[]{:S(2)}) collective-permute-start(bf16[128,512]{1,0:T(8,128)(2,1)S(1)} %copy.106), channel_id=1, source_target_pairs={{0,4},{4,8},{8,12},{12,16},{16,20},{20,24},{24,28},{1,5},{5,9},{9,... | collective-permute-start | bytes 393224 | tf_op jit(solution)/shard_map/while/body/eval_jaxpr/ppermute | solution.py:12
  24.7 6.6 %collective-permute-start.3 = (f32[128,64]{0,1:T(8,128)S(1)}, f32[128,64]{0,1:T(8,128)}, u32[]{:S(2)}, u32[]{:S(2)}) collective-permute-start(f32[128,64]{0,1:T(8,128)S(1)} %get-tuple-element.774), channel_id=1, source_target_pairs={{28,0},{0,4},{4,8},{8,12},{12,16},{16,20},{20,24},{24,28},{29,1},{... | collective-permute-start | bytes 98312 | tf_op jit(solution)/shard_map/while/body/eval_jaxpr/ppermute | solution.py:18
  26.0 6.1 %collective-permute-start.1 = (bf16[128,64]{0,1:T(8,128)(2,1)S(1)}, bf16[128,64]{0,1:T(8,128)(2,1)S(1)}, u32[]{:S(2)}, u32[]{:S(2)}) collective-permute-start(bf16[128,64]{0,1:T(8,128)(2,1)S(1)} %copy.107), channel_id=1, source_target_pairs={{0,4},{4,8},{8,12},{12,16},{16,20},{20,24},{24,28},{1,5},{5,9},{9,... | collective-permute-start | bytes 49160 | tf_op jit(solution)/shard_map/while/body/eval_jaxpr/ppermute | solution.py:12
  32.2 15.7 %collective-permute-start.2 = (f32[128,512]{1,0:T(8,128)S(1)}, f32[128,512]{1,0:T(8,128)S(1)}, u32[]{:S(2)}, u32[]{:S(2)}) collective-permute-start(f32[128,512]{1,0:T(8,128)S(1)} %get-tuple-element.773), channel_id=1, source_target_pairs={{28,0},{0,4},{4,8},{8,12},{12,16},{16,20},{20,24},{24,28},{29,1},{... | collective-permute-start | bytes 786440 | tf_op jit(solution)/shard_map/while/body/eval_jaxpr/ppermute | solution.py:18
  36.9 11.0 %collective-permute-start = (bf16[128,512]{1,0:T(8,128)(2,1)S(1)}, bf16[128,512]{1,0:T(8,128)(2,1)S(1)}, u32[]{:S(2)}, u32[]{:S(2)}) collective-permute-start(bf16[128,512]{1,0:T(8,128)(2,1)S(1)} %copy.106), channel_id=1, source_target_pairs={{0,4},{4,8},{8,12},{12,16},{16,20},{20,24},{24,28},{1,5},{5,9},{9,... | collective-permute-start | bytes 393224 | tf_op jit(solution)/shard_map/while/body/eval_jaxpr/ppermute | solution.py:12
  41.0 6.2 %collective-permute-start.3 = (f32[128,64]{0,1:T(8,128)S(1)}, f32[128,64]{0,1:T(8,128)}, u32[]{:S(2)}, u32[]{:S(2)}) collective-permute-start(f32[128,64]{0,1:T(8,128)S(1)} %get-tuple-element.774), channel_id=1, source_target_pairs={{28,0},{0,4},{4,8},{8,12},{12,16},{16,20},{20,24},{24,28},{29,1},{... | collective-permute-start | bytes 98312 | tf_op jit(solution)/shard_map/while/body/eval_jaxpr/ppermute | solution.py:18
  41.3 6.6 %collective-permute-start.1 = (bf16[128,64]{0,1:T(8,128)(2,1)S(1)}, bf16[128,64]{0,1:T(8,128)(2,1)S(1)}, u32[]{:S(2)}, u32[]{:S(2)}) collective-permute-start(bf16[128,64]{0,1:T(8,128)(2,1)S(1)} %copy.107), channel_id=1, source_target_pairs={{0,4},{4,8},{8,12},{12,16},{16,20},{20,24},{24,28},{1,5},{5,9},{9,... | collective-permute-start | bytes 49160 | tf_op jit(solution)/shard_map/while/body/eval_jaxpr/ppermute | solution.py:12
  48.1 14.4 %collective-permute-start.2 = (f32[128,512]{1,0:T(8,128)S(1)}, f32[128,512]{1,0:T(8,128)S(1)}, u32[]{:S(2)}, u32[]{:S(2)}) collective-permute-start(f32[128,512]{1,0:T(8,128)S(1)} %get-tuple-element.773), channel_id=1, source_target_pairs={{28,0},{0,4},{4,8},{8,12},{12,16},{16,20},{20,24},{24,28},{29,1},{... | collective-permute-start | bytes 786440 | tf_op jit(solution)/shard_map/while/body/eval_jaxpr/ppermute | solution.py:18
  48.6 14.0 %collective-permute-start = (bf16[128,512]{1,0:T(8,128)(2,1)S(1)}, bf16[128,512]{1,0:T(8,128)(2,1)S(1)}, u32[]{:S(2)}, u32[]{:S(2)}) collective-permute-start(bf16[128,512]{1,0:T(8,128)(2,1)S(1)} %copy.106), channel_id=1, source_target_pairs={{0,4},{4,8},{8,12},{12,16},{16,20},{20,24},{24,28},{1,5},{5,9},{9,... | collective-permute-start | bytes 393224 | tf_op jit(solution)/shard_map/while/body/eval_jaxpr/ppermute | solution.py:12
  56.2 5.6 %collective-permute-start.3 = (f32[128,64]{0,1:T(8,128)S(1)}, f32[128,64]{0,1:T(8,128)}, u32[]{:S(2)}, u32[]{:S(2)}) collective-permute-start(f32[128,64]{0,1:T(8,128)S(1)} %get-tuple-element.774), channel_id=1, source_target_pairs={{28,0},{0,4},{4,8},{8,12},{12,16},{16,20},{20,24},{24,28},{29,1},{... | collective-permute-start | bytes 98312 | tf_op jit(solution)/shard_map/while/body/eval_jaxpr/ppermute | solution.py:18
  56.3 6.2 %collective-permute-start.1 = (bf16[128,64]{0,1:T(8,128)(2,1)S(1)}, bf16[128,64]{0,1:T(8,128)(2,1)S(1)}, u32[]{:S(2)}, u32[]{:S(2)}) collective-permute-start(bf16[128,64]{0,1:T(8,128)(2,1)S(1)} %copy.107), channel_id=1, source_target_pairs={{0,4},{4,8},{8,12},{12,16},{16,20},{20,24},{24,28},{1,5},{5,9},{9,... | collective-permute-start | bytes 49160 | tf_op jit(solution)/shard_map/while/body/eval_jaxpr/ppermute | solution.py:12
  62.7 12.6 %collective-permute-start.2 = (f32[128,512]{1,0:T(8,128)S(1)}, f32[128,512]{1,0:T(8,128)S(1)}, u32[]{:S(2)}, u32[]{:S(2)}) collective-permute-start(f32[128,512]{1,0:T(8,128)S(1)} %get-tuple-element.773), channel_id=1, source_target_pairs={{28,0},{0,4},{4,8},{8,12},{12,16},{16,20},{20,24},{24,28},{29,1},{... | collective-permute-start | bytes 786440 | tf_op jit(solution)/shard_map/while/body/eval_jaxpr/ppermute | solution.py:18
  63.8 11.7 %collective-permute-start = (bf16[128,512]{1,0:T(8,128)(2,1)S(1)}, bf16[128,512]{1,0:T(8,128)(2,1)S(1)}, u32[]{:S(2)}, u32[]{:S(2)}) collective-permute-start(bf16[128,512]{1,0:T(8,128)(2,1)S(1)} %copy.106), channel_id=1, source_target_pairs={{0,4},{4,8},{8,12},{12,16},{16,20},{20,24},{24,28},{1,5},{5,9},{9,... | collective-permute-start | bytes 393224 | tf_op jit(solution)/shard_map/while/body/eval_jaxpr/ppermute | solution.py:12
  66.6 8.0 %collective-permute-start.3 = (f32[128,64]{0,1:T(8,128)S(1)}, f32[128,64]{0,1:T(8,128)}, u32[]{:S(2)}, u32[]{:S(2)}) collective-permute-start(f32[128,64]{0,1:T(8,128)S(1)} %get-tuple-element.774), channel_id=1, source_target_pairs={{28,0},{0,4},{4,8},{8,12},{12,16},{16,20},{20,24},{24,28},{29,1},{... | collective-permute-start | bytes 98312 | tf_op jit(solution)/shard_map/while/body/eval_jaxpr/ppermute | solution.py:18
  71.2 4.2 %collective-permute-start.1 = (bf16[128,64]{0,1:T(8,128)(2,1)S(1)}, bf16[128,64]{0,1:T(8,128)(2,1)S(1)}, u32[]{:S(2)}, u32[]{:S(2)}) collective-permute-start(bf16[128,64]{0,1:T(8,128)(2,1)S(1)} %copy.107), channel_id=1, source_target_pairs={{0,4},{4,8},{8,12},{12,16},{16,20},{20,24},{24,28},{1,5},{5,9},{9,... | collective-permute-start | bytes 49160 | tf_op jit(solution)/shard_map/while/body/eval_jaxpr/ppermute | solution.py:12
  75.6 12.5 %collective-permute-start.2 = (f32[128,512]{1,0:T(8,128)S(1)}, f32[128,512]{1,0:T(8,128)S(1)}, u32[]{:S(2)}, u32[]{:S(2)}) collective-permute-start(f32[128,512]{1,0:T(8,128)S(1)} %get-tuple-element.773), channel_id=1, source_target_pairs={{28,0},{0,4},{4,8},{8,12},{12,16},{16,20},{20,24},{24,28},{29,1},{... | collective-permute-start | bytes 786440 | tf_op jit(solution)/shard_map/while/body/eval_jaxpr/ppermute | solution.py:18
  77.3 10.8 %collective-permute-start = (bf16[128,512]{1,0:T(8,128)(2,1)S(1)}, bf16[128,512]{1,0:T(8,128)(2,1)S(1)}, u32[]{:S(2)}, u32[]{:S(2)}) collective-permute-start(bf16[128,512]{1,0:T(8,128)(2,1)S(1)} %copy.106), channel_id=1, source_target_pairs={{0,4},{4,8},{8,12},{12,16},{16,20},{20,24},{24,28},{1,5},{5,9},{9,... | collective-permute-start | bytes 393224 | tf_op jit(solution)/shard_map/while/body/eval_jaxpr/ppermute | solution.py:12
  80.6 6.7 %collective-permute-start.3 = (f32[128,64]{0,1:T(8,128)S(1)}, f32[128,64]{0,1:T(8,128)}, u32[]{:S(2)}, u32[]{:S(2)}) collective-permute-start(f32[128,64]{0,1:T(8,128)S(1)} %get-tuple-element.774), channel_id=1, source_target_pairs={{28,0},{0,4},{4,8},{8,12},{12,16},{16,20},{20,24},{24,28},{29,1},{... | collective-permute-start | bytes 98312 | tf_op jit(solution)/shard_map/while/body/eval_jaxpr/ppermute | solution.py:18
  81.8 6.3 %collective-permute-start.1 = (bf16[128,64]{0,1:T(8,128)(2,1)S(1)}, bf16[128,64]{0,1:T(8,128)(2,1)S(1)}, u32[]{:S(2)}, u32[]{:S(2)}) collective-permute-start(bf16[128,64]{0,1:T(8,128)(2,1)S(1)} %copy.107), channel_id=1, source_target_pairs={{0,4},{4,8},{8,12},{12,16},{16,20},{20,24},{24,28},{1,5},{5,9},{9,... | collective-permute-start | bytes 49160 | tf_op jit(solution)/shard_map/while/body/eval_jaxpr/ppermute | solution.py:12
  88.2 11.4 %collective-permute-start.2 = (f32[128,512]{1,0:T(8,128)S(1)}, f32[128,512]{1,0:T(8,128)S(1)}, u32[]{:S(2)}, u32[]{:S(2)}) collective-permute-start(f32[128,512]{1,0:T(8,128)S(1)} %get-tuple-element.773), channel_id=1, source_target_pairs={{28,0},{0,4},{4,8},{8,12},{12,16},{16,20},{20,24},{24,28},{29,1},{... | collective-permute-start | bytes 786440 | tf_op jit(solution)/shard_map/while/body/eval_jaxpr/ppermute | solution.py:18
  90.5 9.3 %collective-permute-start = (bf16[128,512]{1,0:T(8,128)(2,1)S(1)}, bf16[128,512]{1,0:T(8,128)(2,1)S(1)}, u32[]{:S(2)}, u32[]{:S(2)}) collective-permute-start(bf16[128,512]{1,0:T(8,128)(2,1)S(1)} %copy.106), channel_id=1, source_target_pairs={{0,4},{4,8},{8,12},{12,16},{16,20},{20,24},{24,28},{1,5},{5,9},{9,... | collective-permute-start | bytes 393224 | tf_op jit(solution)/shard_map/while/body/eval_jaxpr/ppermute | solution.py:12
  93.3 5.6 %collective-permute-start.3 = (f32[128,64]{0,1:T(8,128)S(1)}, f32[128,64]{0,1:T(8,128)}, u32[]{:S(2)}, u32[]{:S(2)}) collective-permute-start(f32[128,64]{0,1:T(8,128)S(1)} %get-tuple-element.774), channel_id=1, source_target_pairs={{28,0},{0,4},{4,8},{8,12},{12,16},{16,20},{20,24},{24,28},{29,1},{... | collective-permute-start | bytes 98312 | tf_op jit(solution)/shard_map/while/body/eval_jaxpr/ppermute | solution.py:18
  94.5 5.2 %collective-permute-start.1 = (bf16[128,64]{0,1:T(8,128)(2,1)S(1)}, bf16[128,64]{0,1:T(8,128)(2,1)S(1)}, u32[]{:S(2)}, u32[]{:S(2)}) collective-permute-start(bf16[128,64]{0,1:T(8,128)(2,1)S(1)} %copy.107), channel_id=1, source_target_pairs={{0,4},{4,8},{8,12},{12,16},{16,20},{20,24},{24,28},{1,5},{5,9},{9,... | collective-permute-start | bytes 49160 | tf_op jit(solution)/shard_map/while/body/eval_jaxpr/ppermute | solution.py:12
  99.9 11.6 %collective-permute-start.2 = (f32[128,512]{1,0:T(8,128)S(1)}, f32[128,512]{1,0:T(8,128)S(1)}, u32[]{:S(2)}, u32[]{:S(2)}) collective-permute-start(f32[128,512]{1,0:T(8,128)S(1)} %get-tuple-element.773), channel_id=1, source_target_pairs={{28,0},{0,4},{4,8},{8,12},{12,16},{16,20},{20,24},{24,28},{29,1},{... | collective-permute-start | bytes 786440 | tf_op jit(solution)/shard_map/while/body/eval_jaxpr/ppermute | solution.py:18
  100.1 11.4 %collective-permute-start = (bf16[128,512]{1,0:T(8,128)(2,1)S(1)}, bf16[128,512]{1,0:T(8,128)(2,1)S(1)}, u32[]{:S(2)}, u32[]{:S(2)}) collective-permute-start(bf16[128,512]{1,0:T(8,128)(2,1)S(1)} %copy.106), channel_id=1, source_target_pairs={{0,4},{4,8},{8,12},{12,16},{16,20},{20,24},{24,28},{1,5},{5,9},{9,... | collective-permute-start | bytes 393224 | tf_op jit(solution)/shard_map/while/body/eval_jaxpr/ppermute | solution.py:12
  105.1 5.6 %collective-permute-start.3 = (f32[128,64]{0,1:T(8,128)S(1)}, f32[128,64]{0,1:T(8,128)}, u32[]{:S(2)}, u32[]{:S(2)}) collective-permute-start(f32[128,64]{0,1:T(8,128)S(1)} %get-tuple-element.774), channel_id=1, source_target_pairs={{28,0},{0,4},{4,8},{8,12},{12,16},{16,20},{20,24},{24,28},{29,1},{... | collective-permute-start | bytes 98312 | tf_op jit(solution)/shard_map/while/body/eval_jaxpr/ppermute | solution.py:18
  105.2 6.3 %collective-permute-start.1 = (bf16[128,64]{0,1:T(8,128)(2,1)S(1)}, bf16[128,64]{0,1:T(8,128)(2,1)S(1)}, u32[]{:S(2)}, u32[]{:S(2)}) collective-permute-start(bf16[128,64]{0,1:T(8,128)(2,1)S(1)} %copy.107), channel_id=1, source_target_pairs={{0,4},{4,8},{8,12},{12,16},{16,20},{20,24},{24,28},{1,5},{5,9},{9,... | collective-permute-start | bytes 49160 | tf_op jit(solution)/shard_map/while/body/eval_jaxpr/ppermute | solution.py:12
  111.5 8.5 %collective-permute-start.4 = (f32[128,512]{1,0:T(8,128)S(1)}, f32[128,512]{1,0:T(8,128)S(1)}, u32[]{:S(2)}, u32[]{:S(2)}) collective-permute-start(f32[128,512]{1,0:T(8,128)S(1)} %get-tuple-element.641), channel_id=1, source_target_pairs={{28,0},{0,4},{4,8},{8,12},{12,16},{16,20},{20,24},{24,28},{29,1},{... | collective-permute-start | bytes 786440 | tf_op jit(solution)/shard_map/ppermute | solution.py:18
  120.0 0.7 copy-start.14
  120.0 1.0 copy-start.9
  120.8 75.1 %reduce-scatter.2.cloned.1.call-start = ((), (), s32[]{:S(2)}) async-start(), calls=%async_computation.2 | async-start | bytes 1179648 | tf_op jit(solution)/shard_map/reduce_scatter | solution.py:141
  122.7 1.0 copy-start.7
  122.7 6.2 %collective-permute-start.5 = (f32[128,64]{0,1:T(8,128)S(1)}, f32[128,64]{0,1:T(8,128)S(1)}, u32[]{:S(2)}, u32[]{:S(2)}) collective-permute-start(f32[128,64]{0,1:T(8,128)S(1)} %get-tuple-element.642), channel_id=1, source_target_pairs={{28,0},{0,4},{4,8},{8,12},{12,16},{16,20},{20,24},{24,28},{29,1},{... | collective-permute-start | bytes 98312 | tf_op jit(solution)/shard_map/ppermute | solution.py:18
Sparse Core Ops, SparseCore 0:
  120.9 38.9 all-reduce.1
Sparse Core Ops, SparseCore 1:
  125.2 70.5 reduce-scatter.1
where the time goes:
time: 209 us; the launch traced here: 205 us
  starting transfers between devices  74.4 us (36%)
  waiting for transfers between devices  66.7 us (32%)
  blocking collectives  22.4 us (11%)
  local copies, waits for them, and re-layouts  18.5 us (9%)
  between operations  15.8 us (8%)
  matrix products  4.8 us (2%)
    ppermute x14, starting transfers between devices, shifted(): return lax.ppermute(shard, axis, pairs)  52.9 us
    reduce_scatter x1, waiting for transfers between devices, per_device(): lax.psum_scatter(factor * term.reshape(lax.axis_size('sp') * (lat_width /...  35.9 us
    psum x1, blocking collectives, per_device(): lat_grad, rot_grad = lax.psum((lat_grad, rot_grad), 'tp')  22.4 us
    ppermute x16, waiting for transfers between devices, from_behind(): return lax.ppermute(block, axis, route)  22 us
    ppermute x16, starting transfers between devices, from_behind(): return lax.ppermute(block, axis, route)  21.4 us
    unnamed x39, local copies, waits for them, and re-layouts  9.25 us
    psum x1, waiting for transfers between devices, per_device(): lat_grad, rot_grad = lax.psum((lat_grad, rot_grad), 'tp')  8.66 us
    while x28, local copies, waits for them, and re-layouts  5.53 us
  transfers between devices with their start and end apart: 32, of which 11 were waited for; matrix products, arithmetic and copies ran while one was open for 5% of the time, Pallas kernels for 0%

commit v1 on v0

v1 whole, which is shorter than its diff:
```python
import functools

import jax
import jax.numpy as jnp
from jax import lax
from jax.experimental import pallas as pl
from jax.experimental.pallas import tpu as pltpu
from jax.sharding import PartitionSpec as P

SEQ_DEVICES = 32
MESH = pl.DeviceIdType.MESH
F32 = jnp.float32
BF16 = jnp.bfloat16


def dot(a, b, ca, cb, precision=None):
    return lax.dot_general(
        a, b, (((ca,), (cb,)), ((), ())), preferred_element_type=F32, precision=precision
    )


def kernel(
    dims,
    qm, qr, lat, rot, kw, vw, ho, og, logs,
    o_main, o_rot, o_lat, o_krot, o_kw,
    lat_buf, rot_buf, ql, gr, qrp, mixed, rsum, gpart, obuf, kwst, kwrecv, fin_s, fin_r,
    ksend, krecv, fsend, frecv, finsend, finrecv, agsend, agrecv, kwsend, kwrecvs,
    *halving,
):
    n_sp, n_tp, heads, factor = dims
    stages = n_tp.bit_length() - 1
    half_s, half_r = halving[:stages], halving[stages : 2 * stages]
    half_ss, half_rs = halving[2 * stages : 3 * stages], halving[3 * stages :]
    span = min(SEQ_DEVICES, n_sp)
    lead = span // 4
    tok, width = lat.shape
    rdim = rot.shape[1]
    kdim = kw.shape[1] // heads
    vdim = vw.shape[1] // heads
    sp = lax.axis_index("sp")
    tp = lax.axis_index("tp")
    seq = (sp + lead) // span
    first = jnp.maximum(seq * span - lead, 0)
    last = jnp.minimum((seq + 1) * span - lead, n_sp)
    before = sp - first
    after = last - 1 - sp
    low = tp % 2
    pair = tp + 1 - 2 * low
    half = tok // 2

    barrier = pltpu.get_barrier_semaphore()

    @pl.loop(1, n_sp)
    def _(d):
        pl.semaphore_signal(
            barrier, inc=1, device_id={"sp": (sp + d) % n_sp}, device_id_type=MESH
        )

    for t in range(1, n_tp):
        pl.semaphore_signal(
            barrier, inc=1, device_id={"tp": (tp + t) % n_tp}, device_id_type=MESH
        )
    pl.semaphore_wait(barrier, n_sp - 1 + n_tp - 1)

    mine = pl.ds(pl.multiple_of(low * half, half), half)
    theirs = pl.ds(pl.multiple_of((1 - low) * half, half), half)

    def key_copies(i):
        return [
            pltpu.make_async_remote_copy(
                src_ref=src.at[mine], dst_ref=dst.at[i, mine],
                send_sem=ksend.at[i, n], recv_sem=krecv.at[i, n],
                device_id={"sp": sp + i}, device_id_type=MESH,
            )
            for n, (src, dst) in enumerate(((lat, lat_buf), (rot, rot_buf)))
        ]

    def forward_copies(i, rows):
        return [
            pltpu.make_async_remote_copy(
                src_ref=buf.at[i, rows], dst_ref=buf.at[i, rows],
                send_sem=fsend.at[i, n], recv_sem=frecv.at[i, n],
                device_id={"tp": pair}, device_id_type=MESH,
            )
            for n, buf in enumerate((lat_buf, rot_buf))
        ]

    @pl.loop(1, after + 1)
    def _(i):
        for c in key_copies(i):
            c.start()

    lat_buf[0] = lat[...]
    rot_buf[0] = rot[...]
    terms_parts = []
    for h in range(heads):
        rows = slice(h * tok, (h + 1) * tok)
        kcols = slice(h * kdim, (h + 1) * kdim)
        vcols = slice(h * vdim, (h + 1) * vdim)
        ql[rows] = dot(qm[:, kcols], kw[:, kcols], 1, 1).astype(BF16)
        gr[rows] = dot(og[:, vcols], vw[:, vcols], 1, 1).astype(BF16)
        qrp[rows] = jnp.concatenate(
            [qr[:, h * rdim : (h + 1) * rdim], jnp.zeros((tok, qrp.shape[1] - rdim), BF16)], axis=1
        )
        prod = ho[:, vcols].astype(F32) * og[:, vcols].astype(F32)
        terms_parts.append(
            dot(jnp.ones((8, vdim), F32), prod, 1, 1, lax.Precision.HIGHEST)[0:1]
        )
    terms = jnp.concatenate(terms_parts, axis=1)
    row_logs = jnp.concatenate([logs[h : h + 1, :] for h in range(heads)], axis=1)
    mixed[...] = jnp.zeros_like(mixed)
    rsum[...] = jnp.zeros_like(rsum)

    def level_offset(level):
        off = 0
        for b in range(level):
            off = off + ((tp // (1 << b)) % 2) * (tok >> (b + 1))
        return off

    def half_copy(s, i):
        bit = (tp // (1 << s)) % 2
        return pltpu.make_async_remote_copy(
            src_ref=half_s[s].at[i], dst_ref=half_r[s].at[i],
            send_sem=half_ss[s].at[i], recv_sem=half_rs[s].at[i],
            device_id={"tp": tp + (1 - 2 * bit) * (1 << s)}, device_id_type=MESH,
        )

    def send_half(s, i):
        size = tok >> (s + 1)
        bit = (tp // (1 << s)) % 2
        start = pl.multiple_of(level_offset(s) + (1 - bit) * size, size)
        half_s[s][i] = gpart[i, pl.ds(start, size), :].astype(BF16)
        half_copy(s, i).start()

    def fin_copy(i):
        return pltpu.make_async_remote_copy(
            src_ref=fin_s.at[i], dst_ref=fin_r.at[i],
            send_sem=finsend.at[i], recv_sem=finrecv.at[i],
            device_id={"sp": sp - i}, device_id_type=MESH,
        )

    def arrive(i):
        for c in key_copies(i):
            c.wait_recv()
        for c in forward_copies(i, mine):
            c.start()

    quarter = tok >> stages
    my_rows = pl.ds(pl.multiple_of(level_offset(stages), quarter), quarter)

    def attend(i):
        @pl.when(i < before)
        def _():
            arrive(i + 1)

        @pl.when(i > 0)
        def _():
            for c in forward_copies(i, theirs):
                c.wait_recv()

        lt = lat_buf[i]
        rt = rot_buf[i]
        scores = dot(lt, ql[...], 1, 1) + dot(rt, qrp[:, :rdim], 1, 1)
        weights = jnp.exp(factor * scores - row_logs)
        key_at = lax.broadcasted_iota(jnp.int32, weights.shape, 0)
        query_at = lax.broadcasted_iota(jnp.int32, weights.shape, 1) % tok
        weights = jnp.where((key_at <= query_at) | (i > 0), weights, 0.0)
        slopes = dot(lt, gr[...], 1, 1)
        dscores = weights * (slopes - terms)
        wl = weights.astype(BF16)
        dl = dscores.astype(BF16)
        gpart[i, :, :width] = factor * dot(dl, ql[...], 1, 0) + dot(wl, gr[...], 1, 0)
        gpart[i, :, width:] = factor * dot(dl, qrp[...], 1, 0)
        send_half(0, i)
        mixed[...] += dot(dl, lt, 0, 0)
        rsum[...] += dot(dl, rt, 0, 0)

    @pl.loop(0, before + 1 + stages)
    def _(it):
        @pl.when(it <= before)
        def _():
            attend(it)

        for s in range(1, stages + 1):
            i = it - s

            @pl.when((i >= 0) & (i <= before))
            def _():
                half_copy(s - 1, i).wait_recv()
                size = tok >> s
                rows = pl.ds(pl.multiple_of(level_offset(s), size), size)
                gpart[i, rows, :] += half_r[s - 1][i].astype(F32)
                if s < stages:
                    send_half(s, i)
                else:

                    @pl.when(i > 0)
                    def _():
                        fin_s[i] = gpart[i, rows, :].astype(BF16)
                        fin_copy(i).start()

    part = o_kw.shape[0]

    def kw_copy(d):
        dest = (sp + d) % n_sp
        return pltpu.make_async_remote_copy(
            src_ref=kwst.at[dest], dst_ref=kwrecv.at[n_sp - d],
            send_sem=kwsend.at[d], recv_sem=kwrecvs.at[n_sp - d],
            device_id={"sp": dest}, device_id_type=MESH,
        )

    def kw_landing(d):
        return pltpu.make_async_remote_copy(
            src_ref=kwst.at[0], dst_ref=kwrecv.at[d],
            send_sem=kwsend.at[d], recv_sem=kwrecvs.at[d],
            device_id={"sp": (sp + d) % n_sp}, device_id_type=MESH,
        )

    low_parts = []
    for h in range(heads):
        rows = slice(h * tok, (h + 1) * tok)
        kcols = slice(h * kdim, (h + 1) * kdim)
        ml = mixed[rows].astype(BF16)
        term = (factor * dot(ml, qm[:, kcols], 0, 0)).astype(BF16)
        for d in range(n_sp):
            kwst[d, :, kcols] = term[d * part : (d + 1) * part]
        low_parts.append(ml)

    @pl.loop(1, n_sp)
    def _(d):
        kw_copy(d).start()

    for h in range(heads):
        rows = slice(h * tok, (h + 1) * tok)
        kcols = slice(h * kdim, (h + 1) * kdim)
        o_main[:, kcols] = factor * dot(low_parts[h], kw[:, kcols], 1, 0)
        o_rot[:, h * rdim : (h + 1) * rdim] = factor * rsum[rows]

    @pl.loop(1, after + 1)
    def _(i):
        pltpu.make_async_remote_copy(
            src_ref=fin_s.at[i], dst_ref=fin_r.at[i],
            send_sem=finsend.at[i], recv_sem=finrecv.at[i],
            device_id={"sp": sp + i}, device_id_type=MESH,
        ).wait_recv()
        gpart[0, my_rows, :] += fin_r[i].astype(F32)

    obuf[my_rows] = gpart[0, my_rows, :]

    def ag_copy(t):
        return pltpu.make_async_remote_copy(
            src_ref=obuf.at[my_rows], dst_ref=obuf.at[my_rows],
            send_sem=agsend.at[t], recv_sem=agrecv.at[n_tp - t],
            device_id={"tp": (tp + t) % n_tp}, device_id_type=MESH,
        )

    for t in range(1, n_tp):
        ag_copy(t).start()

    total = kwst[sp].astype(F32)
    for d in range(1, n_sp):
        kw_landing(d).wait_recv()
        total = total + kwrecv[d].astype(F32)
    o_kw[...] = total

    for t in range(1, n_tp):
        peer = (tp + t) % n_tp
        off = 0
        for b in range(stages):
            off = off + ((peer // (1 << b)) % 2) * (tok >> (b + 1))
        rows = pl.ds(pl.multiple_of(off, quarter), quarter)
        pltpu.make_async_remote_copy(
            src_ref=obuf.at[rows], dst_ref=obuf.at[rows],
            send_sem=agsend.at[t], recv_sem=agrecv.at[t],
            device_id={"tp": peer}, device_id_type=MESH,
        ).wait_recv()
    o_lat[...] = obuf[:, :width]
    o_krot[...] = obuf[:, width : width + rdim]

    @pl.loop(1, after + 1)
    def _(i):
        for c in key_copies(i):
            c.wait_send()

    @pl.loop(0, before + 1)
    def _(i):
        for s in range(stages):
            half_copy(s, i).wait_send()

        @pl.when(i > 0)
        def _():
            for c in forward_copies(i, mine):
                c.wait_send()
            fin_copy(i).wait_send()

    @pl.loop(1, n_sp)
    def _(d):
        kw_copy(d).wait_send()

    for t in range(1, n_tp):
        ag_copy(t).wait_send()


def per_device(mesh_dims, *args):
    n_sp, n_tp = mesh_dims
    qm, qr, lat, rot, kw, vw, ho, og, logs = args
    heads, tok = logs.shape
    width, rdim = lat.shape[1], rot.shape[1]
    factor = (kw.shape[1] // heads + rdim) ** (-0.5)
    span = min(SEQ_DEVICES, n_sp)
    stages = n_tp.bit_length() - 1
    rpad = -(-rdim // 128) * 128
    wide = width + rpad
    quarter = tok >> stages
    part = width // n_sp
    dma = pltpu.SemaphoreType.DMA
    scratch = [
        pltpu.VMEM((span, tok, width), BF16),
        pltpu.VMEM((span, tok, rdim), BF16),
        pltpu.VMEM((heads * tok, width), BF16),
        pltpu.VMEM((heads * tok, width), BF16),
        pltpu.VMEM((heads * tok, rpad), BF16),
        pltpu.VMEM((heads * tok, width), F32),
        pltpu.VMEM((heads * tok, rdim), F32),
        pltpu.VMEM((span, tok, wide), F32),
        pltpu.VMEM((tok, wide), F32),
        pltpu.VMEM((n_sp, part, kw.shape[1]), BF16),
        pltpu.VMEM((n_sp, part, kw.shape[1]), BF16),
        pltpu.VMEM((span, quarter, wide), BF16),
        pltpu.VMEM((span, quarter, wide), BF16),
        dma((span, 2)), dma((span, 2)), dma((span, 2)), dma((span, 2)),
        dma((span,)), dma((span,)), dma((n_tp,)), dma((n_tp,)), dma((n_sp,)), dma((n_sp,)),
    ]
    halves = [pltpu.VMEM((span, tok >> (s + 1), wide), BF16) for s in range(stages)]
    sems = [dma((span,)) for s in range(stages)]
    scratch = scratch + halves + halves + sems + sems
    outs = (
        jax.ShapeDtypeStruct((tok, kw.shape[1]), F32),
        jax.ShapeDtypeStruct((tok, heads * rdim), F32),
        jax.ShapeDtypeStruct((tok, width), F32),
        jax.ShapeDtypeStruct((tok, rdim), F32),
        jax.ShapeDtypeStruct((part, kw.shape[1]), F32),
    )
    vmem = pl.BlockSpec(memory_space=pltpu.VMEM)
    return pl.pallas_call(
        functools.partial(kernel, (n_sp, n_tp, heads, factor)),
        out_shape=outs,
        in_specs=[vmem] * len(args),
        out_specs=[vmem] * len(outs),
        scratch_shapes=scratch,
        compiler_params=pltpu.CompilerParams(collective_id=0, has_side_effects=True),
        name="latent_attention_backward",
    )(*args)


def solution(mesh):
    dims = (mesh.shape["sp"], mesh.shape["tp"])
    return jax.shard_map(
        functools.partial(per_device, dims),
        mesh=mesh,
        in_specs=(
            P("sp", "tp"),
            P("sp", "tp"),
            P("sp", None),
            P("sp", None),
            P(None, "tp"),
            P(None, "tp"),
            P("sp", "tp"),
            P("sp", "tp"),
            P("tp", "sp"),
        ),
        out_specs=(P("sp", "tp"), P("sp", "tp"), P("sp", None), P("sp", None), P("sp", "tp")),
        check_vma=False,
    )
```

time: 209 us -> 44 us (0.21); the launches traced: 205 us -> 43.7 us
  starting transfers between devices: 74.4 us -> 0 us
  waiting for transfers between devices: 66.7 us -> 0 us
  Pallas kernels: 0 us -> 35.8 us
  blocking collectives: 22.4 us -> 0 us
  between operations: 15.8 us -> 0.64 us
  local copies, waits for them, and re-layouts: 18.5 us -> 7.33 us
  matrix products: 4.8 us -> 0 us
    ppermute x30 -> x0, starting transfers between devices: 74.4 us -> none  [the longest x14 52.9 us: shifted(): return lax.ppermute(shard, axis, pairs)]
    reduce_scatter x1 -> x0, waiting for transfers between devices: 35.9 us -> none  [per_device(): lax.psum_scatter(factor * term.reshape(lax.axis_size('sp') * (lat_width /...]
    pallas_call x0 -> x1, Pallas kernels: none -> 35.8 us  [per_device(): pl.pallas_call(functools.partial(kernel, (n_sp, n_tp, heads, factor)), ou...]
    psum x1 -> x0, blocking collectives: 22.4 us -> none  [per_device(): lat_grad, rot_grad = lax.psum((lat_grad, rot_grad), 'tp')]
    ppermute x30 -> x0, waiting for transfers between devices: 22.1 us -> none  [the longest x16 22 us: from_behind(): return lax.ppermute(block, axis, route)]
    psum x1 -> x0, waiting for transfers between devices: 8.66 us -> none  [per_device(): lat_grad, rot_grad = lax.psum((lat_grad, rot_grad), 'tp')]
    while x28 -> x0, local copies, waits for them, and re-layouts: 5.53 us -> none
    dot_general x12 -> x0, matrix products: 4.8 us -> none  [the longest x1 1.74 us: attend_block(): jnp.einsum('thk,kr->thr', dscores_low, rot_block, preferred_element_type=...]
  transfers between devices with their start and end apart: 32 -> 0, of which waited for: 11 -> 0; matrix products, arithmetic and copies ran while one was open for 5% -> 0% of each run, Pallas kernels for 0% -> 0%
where the time goes in v1:
time: 44 us; the launch traced here: 43.7 us
  Pallas kernels  35.8 us (81%)
  local copies, waits for them, and re-layouts  7.33 us (17%)
  between operations  0.64 us (1%)
    pallas_call x1, Pallas kernels, per_device(): pl.pallas_call(functools.partial(kernel, (n_sp, n_tp, heads, factor)), ou...  35.8 us
    unnamed x11, local copies, waits for them, and re-layouts  5.79 us
    pallas_call x1, local copies, waits for them, and re-layouts, per_device(): pl.pallas_call(functools.partial(kernel, (n_sp, n_tp, heads, factor)), ou...  1.54 us

profile of v1, /device:TPU:1, one launch (start us, length us, event | category | flops | bytes accessed | tf_op | source)
XLA Modules:
  0.0 43.7 jit_solution(16333883414884666339)
XLA Ops:
  0.6 1.4 %copy.14.rot = bf16[128,64]{1,0:T(8,128)(2,1)} copy(bf16[128,64]{0,1:T(8,128)(2,1)} %param.12) | data formatting | bytes 32768 | tf_op args[3]
  2.1 35.8 %latent_attention_backward.1 = (f32[128,512]{1,0:T(8,128)}, f32[128,256]{1,0:T(8,128)}, f32[128,512]{1,0:T(8,128)}, f32[128,64]{1,0:T(8,128)}, f32[64,512]{1,0:T(8,128)}) custom-call(bf16[128,512]{1,0:T(8,128)(2,1)} %qm.1, bf16[128,256]{1,0:T(8,128)(2,1)} %qr.1, bf16[128,512]{1,0:T(8,128)(2,1)} %lat.1, bf16[128,64]{1,0:T(8,128)(2,1)} %copy.14.rot, ...), custom_call_target="tpu_custom_call" | custom-call | tf_op jit(solution)/shard_map/latent_attention_backward/pallas_call | solution.py:345
  37.8 1.5 %copy.15 = f32[128,64]{0,1:T(8,128)} copy(f32[128,64]{1,0:T(8,128)} %get-tuple-element.8) | data formatting | bytes 65536 | tf_op jit(solution)/shard_map/latent_attention_backward/pallas_call | solution.py:345
  39.4 0.0 copy-start.2
  39.4 1.7 %copy.20 = f32[128,512]{1,0:T(8,128)} copy(f32[128,512]{1,0:T(8,128)} %get-tuple-element.15) | data formatting | bytes 524288
  41.1 0.0 copy-done.2
  41.1 0.0 copy-start
  41.1 0.7 %copy.21 = f32[128,256]{1,0:T(8,128)} copy(f32[128,256]{1,0:T(8,128)S(1)} %copy-done.2) | data formatting | bytes 262144
  41.7 0.3 copy-done
  42.1 0.0 copy-start.1
  42.1 0.7 %copy.22 = f32[128,512]{1,0:T(8,128)} copy(f32[128,512]{1,0:T(8,128)S(1)} %copy-done) | data formatting | bytes 524288
  42.8 0.3 copy-done.1
  43.1 0.7 %copy.23 = f32[64,512]{1,0:T(8,128)} copy(f32[64,512]{1,0:T(8,128)S(1)} %copy-done.1) | data formatting | bytes 262144
Async XLA Ops:
  39.4 1.7 %copy-start.2 = (f32[128,256]{1,0:T(8,128)S(1)}, f32[128,256]{1,0:T(8,128)}, u32[]{:S(2)}) copy-start(f32[128,256]{1,0:T(8,128)} %get-tuple-element.16) | copy-start | bytes 393220
  41.1 1.0 %copy-start = (f32[128,512]{1,0:T(8,128)S(1)}, f32[128,512]{1,0:T(8,128)}, u32[]{:S(2)}) copy-start(f32[128,512]{1,0:T(8,128)} %get-tuple-element.17) | copy-start | bytes 786436
  42.1 1.0 %copy-start.1 = (f32[64,512]{1,0:T(8,128)S(1)}, f32[64,512]{1,0:T(8,128)}, u32[]{:S(2)}) copy-start(f32[64,512]{1,0:T(8,128)} %get-tuple-element.19) | copy-start | bytes 393220

commit v2 on v1

--- a/solution.py
+++ b/solution.py
@@ -1,4 +1,5 @@
 import functools
+import math
 
 import jax
 import jax.numpy as jnp
@@ -8,6 +9,7 @@
 from jax.sharding import PartitionSpec as P
 
 SEQ_DEVICES = 32
+VMEM_BYTES = 67043328
 MESH = pl.DeviceIdType.MESH
 F32 = jnp.float32
 BF16 = jnp.bfloat16
@@ -21,8 +23,9 @@
 
 def kernel(
     dims,
-    qm, qr, lat, rot, kw, vw, ho, og, logs,
+    qm_h, qr_h, lat_h, rot_h, kw_h, vw_h, ho_h, og_h, logs_h,
     o_main, o_rot, o_lat, o_krot, o_kw,
+    qm, qr, lat, rot, kw, vw, ho, og, logs, insem,
     lat_buf, rot_buf, ql, gr, qrp, mixed, rsum, gpart, obuf, kwst, kwrecv, fin_s, fin_r,
     ksend, krecv, fsend, frecv, finsend, finrecv, agsend, agrecv, kwsend, kwrecvs,
     *halving,
@@ -34,9 +37,20 @@
     span = min(SEQ_DEVICES, n_sp)
     lead = span // 4
     tok, width = lat.shape
-    rdim = rot.shape[1]
+    rdim = rot.shape[0]
     kdim = kw.shape[1] // heads
     vdim = vw.shape[1] // heads
+    loads = [
+        pltpu.make_async_copy(src, dst, insem.at[n])
+        for n, (src, dst) in enumerate(
+            (
+                (lat_h, lat), (rot_h, rot), (qm_h, qm), (kw_h, kw), (og_h, og), (vw_h, vw),
+                (ho_h, ho), (qr_h, qr), (logs_h, logs),
+            )
+        )
+    ]
+    for c in loads:
+        c.start()
     sp = lax.axis_index("sp")
     tp = lax.axis_index("tp")
     seq = (sp + lead) // span
@@ -46,7 +60,6 @@
     after = last - 1 - sp
     low = tp % 2
     pair = tp + 1 - 2 * low
-    half = tok // 2
 
     barrier = pltpu.get_barrier_semaphore()
 
@@ -62,28 +75,33 @@
         )
     pl.semaphore_wait(barrier, n_sp - 1 + n_tp - 1)
 
-    mine = pl.ds(pl.multiple_of(low * half, half), half)
-    theirs = pl.ds(pl.multiple_of((1 - low) * half, half), half)
+    def part_of(side, size):
+        return pl.ds(pl.multiple_of(side * (size // 2), size // 2), size // 2)
+
+    keys = ((lat, lat_buf, tok), (rot, rot_buf, rdim))
 
     def key_copies(i):
         return [
             pltpu.make_async_remote_copy(
-                src_ref=src.at[mine], dst_ref=dst.at[i, mine],
+                src_ref=src.at[part_of(low, size)], dst_ref=dst.at[i, part_of(low, size)],
                 send_sem=ksend.at[i, n], recv_sem=krecv.at[i, n],
                 device_id={"sp": sp + i}, device_id_type=MESH,
             )
-            for n, (src, dst) in enumerate(((lat, lat_buf), (rot, rot_buf)))
+            for n, (src, dst, size) in enumerate(keys)
         ]
 
-    def forward_copies(i, rows):
+    def forward_copies(i, side):
         return [
             pltpu.make_async_remote_copy(
-                src_ref=buf.at[i, rows], dst_ref=buf.at[i, rows],
+                src_ref=buf.at[i, part_of(side, size)], dst_ref=buf.at[i, part_of(side, size)],
                 send_sem=fsend.at[i, n], recv_sem=frecv.at[i, n],
                 device_id={"tp": pair}, device_id_type=MESH,
             )
-            for n, buf in enumerate((lat_buf, rot_buf))
+            for n, (_, buf, size) in enumerate(keys)
         ]
+
+    loads[0].wait()
+    loads[1].wait()
 
     @pl.loop(1, after + 1)
     def _(i):
@@ -92,6 +110,8 @@
 
     lat_buf[0] = lat[...]
     rot_buf[0] = rot[...]
+    for c in loads[2:]:
+        c.wait()
     terms_parts = []
     for h in range(heads):
         rows = slice(h * tok, (h + 1) * tok)
@@ -142,7 +162,7 @@
     def arrive(i):
         for c in key_copies(i):
             c.wait_recv()
-        for c in forward_copies(i, mine):
+        for c in forward_copies(i, low):
             c.start()
 
     quarter = tok >> stages
@@ -155,12 +175,12 @@
 
         @pl.when(i > 0)
         def _():
-            for c in forward_copies(i, theirs):
+            for c in forward_copies(i, 1 - low):
                 c.wait_recv()
 
         lt = lat_buf[i]
         rt = rot_buf[i]
-        scores = dot(lt, ql[...], 1, 1) + dot(rt, qrp[:, :rdim], 1, 1)
+        scores = dot(lt, ql[...], 1, 1) + dot(rt, qrp[:, :rdim], 0, 1)
         weights = jnp.exp(factor * scores - row_logs)
         key_at = lax.broadcasted_iota(jnp.int32, weights.shape, 0)
         query_at = lax.broadcasted_iota(jnp.int32, weights.shape, 1) % tok
@@ -173,7 +193,7 @@
         gpart[i, :, width:] = factor * dot(dl, qrp[...], 1, 0)
         send_half(0, i)
         mixed[...] += dot(dl, lt, 0, 0)
-        rsum[...] += dot(dl, rt, 0, 0)
+        rsum[...] += dot(dl, rt, 0, 1)
 
     @pl.loop(0, before + 1 + stages)
     def _(it):
@@ -275,7 +295,7 @@
             device_id={"tp": peer}, device_id_type=MESH,
         ).wait_recv()
     o_lat[...] = obuf[:, :width]
-    o_krot[...] = obuf[:, width : width + rdim]
+    o_krot[...] = obuf[:, width:].T[:rdim]
 
     @pl.loop(1, after + 1)
     def _(i):
@@ -289,7 +309,7 @@
 
         @pl.when(i > 0)
         def _():
-            for c in forward_copies(i, mine):
+            for c in forward_copies(i, low):
                 c.wait_send()
             fin_copy(i).wait_send()
 
@@ -299,6 +319,18 @@
 
     for t in range(1, n_tp):
         ag_copy(t).wait_send()
+
+
+def store(*refs):
+    *pairs, sem = refs
+    count = len(pairs) // 2
+    copies = [
+        pltpu.make_async_copy(pairs[n], pairs[count + n], sem.at[n]) for n in range(count)
+    ]
+    for c in copies:
+        c.start()
+    for c in copies:
+        c.wait()
 
 
 def per_device(mesh_dims, *args):
@@ -306,6 +338,7 @@
     qm, qr, lat, rot, kw, vw, ho, og, logs = args
     heads, tok = logs.shape
     width, rdim = lat.shape[1], rot.shape[1]
+    args = (qm, qr, lat, rot.T, kw, vw, ho, og, logs)
     factor = (kw.shape[1] // heads + rdim) ** (-0.5)
     span = min(SEQ_DEVICES, n_sp)
     stages = n_tp.bit_length() - 1
@@ -314,9 +347,10 @@
     quarter = tok >> stages
     part = width // n_sp
     dma = pltpu.SemaphoreType.DMA
-    scratch = [
+    scratch = [pltpu.VMEM(a.shape, a.dtype) for a in args] + [
+        dma((len(args),)),
         pltpu.VMEM((span, tok, width), BF16),
-        pltpu.VMEM((span, tok, rdim), BF16),
+        pltpu.VMEM((span, rdim, tok), BF16),
         pltpu.VMEM((heads * tok, width), BF16),
         pltpu.VMEM((heads * tok, width), BF16),
         pltpu.VMEM((heads * tok, rpad), BF16),
@@ -334,23 +368,33 @@
     halves = [pltpu.VMEM((span, tok >> (s + 1), wide), BF16) for s in range(stages)]
     sems = [dma((span,)) for s in range(stages)]
     scratch = scratch + halves + halves + sems + sems
-    outs = (
-        jax.ShapeDtypeStruct((tok, kw.shape[1]), F32),
-        jax.ShapeDtypeStruct((tok, heads * rdim), F32),
-        jax.ShapeDtypeStruct((tok, width), F32),
-        jax.ShapeDtypeStruct((tok, rdim), F32),
-        jax.ShapeDtypeStruct((part, kw.shape[1]), F32),
+    shapes = (
+        (tok, kw.shape[1]), (tok, heads * rdim), (tok, width), (rdim, tok), (part, kw.shape[1]),
     )
+    results = sum(4 * math.prod(s) for s in shapes)
     vmem = pl.BlockSpec(memory_space=pltpu.VMEM)
-    return pl.pallas_call(
+    hbm = pl.BlockSpec(memory_space=pltpu.HBM)
+    held = pl.pallas_call(
         functools.partial(kernel, (n_sp, n_tp, heads, factor)),
-        out_shape=outs,
-        in_specs=[vmem] * len(args),
-        out_specs=[vmem] * len(outs),
+        out_shape=[pltpu.VMEM(s, F32) for s in shapes],
+        in_specs=[hbm] * len(args),
+        out_specs=[vmem] * len(shapes),
         scratch_shapes=scratch,
-        compiler_params=pltpu.CompilerParams(collective_id=0, has_side_effects=True),
+        compiler_params=pltpu.CompilerParams(
+            collective_id=0, has_side_effects=True, vmem_limit_bytes=VMEM_BYTES - results - (16 << 10)
+        ),
         name="latent_attention_backward",
     )(*args)
+    main, rotary, lat_out, rot_out, weight = pl.pallas_call(
+        store,
+        out_shape=[jax.ShapeDtypeStruct(s, F32) for s in shapes],
+        in_specs=[vmem] * len(shapes),
+        out_specs=[hbm] * len(shapes),
+        scratch_shapes=[dma((len(shapes),))],
+        compiler_params=pltpu.CompilerParams(vmem_limit_bytes=4 << 20),
+        name="store_outputs",
+    )(*held)
+    return main, rotary, lat_out, rot_out.T, weight
 
 
 def solution(mesh):

time: 44 us -> 34.9 us (0.79)
  local copies, waits for them, and re-layouts: 7.33 us -> 0 us
  Pallas kernels: 35.8 us -> 34.1 us
    unnamed x11 -> x0, local copies, waits for them, and re-layouts: 5.79 us -> none
    pallas_call x1, Pallas kernels: 35.8 us -> 33.1 us  [per_device(): pl.pallas_call(functools.partial(kernel, (n_sp, n_tp, heads, factor)), ou...]
    pallas_call x1 -> x0, local copies, waits for them, and re-layouts: 1.54 us -> none  [per_device(): pl.pallas_call(functools.partial(kernel, (n_sp, n_tp, heads, factor)), ou...]
    pallas_call x0 -> x1, Pallas kernels: none -> 0.93 us  [per_device(): pl.pallas_call(store, out_shape=[jax.ShapeDtypeStruct(s, F32) for s in sh...]
where the time goes in v2:
time: 34.9 us; the launch traced here: 34.7 us
  Pallas kernels  34.1 us (98%)
  between operations  0.64 us (2%)
    pallas_call x1, Pallas kernels, per_device(): pl.pallas_call(functools.partial(kernel, (n_sp, n_tp, heads, factor)), ou...  33.1 us
    pallas_call x1, Pallas kernels, per_device(): pl.pallas_call(store, out_shape=[jax.ShapeDtypeStruct(s, F32) for s in sh...  0.93 us

profile of v2, /device:TPU:1, one launch (start us, length us, event | category | flops | bytes accessed | tf_op | source)
XLA Modules:
  0.0 34.7 jit_solution(5373640195182003606)
XLA Ops:
  0.6 33.1 %latent_attention_backward.1 = (f32[128,512]{1,0:T(8,128)S(1)}, f32[128,256]{1,0:T(8,128)S(1)}, f32[128,512]{1,0:T(8,128)S(1)}, f32[64,128]{1,0:T(8,128)S(1)}, f32[64,512]{1,0:T(8,128)S(1)}) custom-call(bf16[128,512]{1,0:T(8,128)(2,1)} %qm_h.1, bf16[128,256]{1,0:T(8,128)(2,1)} %qr_h.1, bf16[128,512]{1,0:T(8,128)(2,1)} %lat_h.1, bf16[64,128]{1,0:T(8,128)(2,1)} %bitcast.2, ...), custom_call_target="tpu_custom_call" | custom-call | tf_op jit(solution)/shard_map/latent_attention_backward/pallas_call | solution.py:377
  33.8 0.9 %store_outputs.1 = (f32[128,512]{1,0:T(8,128)}, f32[128,256]{1,0:T(8,128)}, f32[128,512]{1,0:T(8,128)}, f32[64,128]{1,0:T(8,128)}, f32[64,512]{1,0:T(8,128)}) custom-call(f32[128,512]{1,0:T(8,128)S(1)} %get-tuple-element.15.refs_0_, f32[128,256]{1,0:T(8,128)S(1)} %get-tuple-element.16.refs_1_, f32[128,512]{1,0:T(8,128)S(1)} %get-tuple-element.17.refs_2_, ...), custom_call_target="tpu_custom_call" | custom-call | tf_op jit(solution)/shard_map/store_outputs/pallas_call | solution.py:388

commit v3 on v2

--- a/solution.py
+++ b/solution.py
@@ -73,7 +73,6 @@
         pl.semaphore_signal(
             barrier, inc=1, device_id={"tp": (tp + t) % n_tp}, device_id_type=MESH
         )
-    pl.semaphore_wait(barrier, n_sp - 1 + n_tp - 1)
 
     def part_of(side, size):
         return pl.ds(pl.multiple_of(side * (size // 2), size // 2), size // 2)
@@ -100,24 +99,27 @@
             for n, (_, buf, size) in enumerate(keys)
         ]
 
-    loads[0].wait()
-    loads[1].wait()
+    for c in loads[:4]:
+        c.wait()
+    lat_buf[0] = lat[...]
+    rot_buf[0] = rot[...]
+    for h in range(heads):
+        kcols = slice(h * kdim, (h + 1) * kdim)
+        ql[h * tok : (h + 1) * tok] = dot(qm[:, kcols], kw[:, kcols], 1, 1).astype(BF16)
+    pl.semaphore_wait(barrier, n_sp - 1 + n_tp - 1)
 
     @pl.loop(1, after + 1)
     def _(i):
         for c in key_copies(i):
             c.start()
 
-    lat_buf[0] = lat[...]
-    rot_buf[0] = rot[...]
-    for c in loads[2:]:
+    for c in loads[4:]:
         c.wait()
     terms_parts = []
     for h in range(heads):
         rows = slice(h * tok, (h + 1) * tok)
         kcols = slice(h * kdim, (h + 1) * kdim)
         vcols = slice(h * vdim, (h + 1) * vdim)
-        ql[rows] = dot(qm[:, kcols], kw[:, kcols], 1, 1).astype(BF16)
         gr[rows] = dot(og[:, vcols], vw[:, vcols], 1, 1).astype(BF16)
         qrp[rows] = jnp.concatenate(
             [qr[:, h * rdim : (h + 1) * rdim], jnp.zeros((tok, qrp.shape[1] - rdim), BF16)], axis=1
@@ -128,8 +130,12 @@
         )
     terms = jnp.concatenate(terms_parts, axis=1)
     row_logs = jnp.concatenate([logs[h : h + 1, :] for h in range(heads)], axis=1)
-    mixed[...] = jnp.zeros_like(mixed)
-    rsum[...] = jnp.zeros_like(rsum)
+
+    @pl.when(before % 2 == 1)
+    def _():
+        lat_buf[before + 1] = jnp.zeros((tok, width), BF16)
+        rot_buf[before + 1] = jnp.zeros((rdim, tok), BF16)
+
 
     def level_offset(level):
         off = 0
@@ -168,56 +174,79 @@
     quarter = tok >> stages
     my_rows = pl.ds(pl.multiple_of(level_offset(stages), quarter), quarter)
 
-    def attend(i):
-        @pl.when(i < before)
+    def pass_on(s, i):
+        @pl.when((i >= 0) & (i <= before))
         def _():
-            arrive(i + 1)
-
-        @pl.when(i > 0)
-        def _():
-            for c in forward_copies(i, 1 - low):
-                c.wait_recv()
-
-        lt = lat_buf[i]
-        rt = rot_buf[i]
+            half_copy(s - 1, i).wait_recv()
+            size = tok >> s
+            rows = pl.ds(pl.multiple_of(level_offset(s), size), size)
+            gpart[i, rows, :] += half_r[s - 1][i].astype(F32)
+            if s < stages:
+                send_half(s, i)
+            else:
+
+                @pl.when(i > 0)
+                def _():
+                    fin_s[i] = gpart[i, rows, :].astype(BF16)
+                    fin_copy(i).start()
+
+    def attend(i, count):
+        if count:
+            for b in range(count):
+
+                @pl.when(i + b <= before)
+                def _(b=b):
+                    for c in forward_copies(i + b, 1 - low):
+                        c.wait_recv()
+
+        size = max(count, 1)
+        lt = lat_buf[pl.ds(i, size)].reshape(size * tok, width)
+        rt = jnp.concatenate([rot_buf[i + b] for b in range(size)], axis=1)
         scores = dot(lt, ql[...], 1, 1) + dot(rt, qrp[:, :rdim], 0, 1)
         weights = jnp.exp(factor * scores - row_logs)
-        key_at = lax.broadcasted_iota(jnp.int32, weights.shape, 0)
-        query_at = lax.broadcasted_iota(jnp.int32, weights.shape, 1) % tok
-        weights = jnp.where((key_at <= query_at) | (i > 0), weights, 0.0)
+        if not count:
+            key_at = lax.broadcasted_iota(jnp.int32, weights.shape, 0)
+            query_at = lax.broadcasted_iota(jnp.int32, weights.shape, 1) % tok
+            weights = jnp.where(key_at <= query_at, weights, 0.0)
         slopes = dot(lt, gr[...], 1, 1)
         dscores = weights * (slopes - terms)
         wl = weights.astype(BF16)
         dl = dscores.astype(BF16)
-        gpart[i, :, :width] = factor * dot(dl, ql[...], 1, 0) + dot(wl, gr[...], 1, 0)
-        gpart[i, :, width:] = factor * dot(dl, qrp[...], 1, 0)
-        send_half(0, i)
-        mixed[...] += dot(dl, lt, 0, 0)
-        rsum[...] += dot(dl, rt, 0, 1)
-
-    @pl.loop(0, before + 1 + stages)
+        part_lat = factor * dot(dl, ql[...], 1, 0) + dot(wl, gr[...], 1, 0)
+        part_rot = factor * dot(dl, qrp[...], 1, 0)
+        gpart[pl.ds(i, size), :, :width] = part_lat.reshape(size, tok, width)
+        gpart[pl.ds(i, size), :, width:] = part_rot.reshape(size, tok, part_rot.shape[1])
+        for b in range(size):
+
+            @pl.when(i + b <= before)
+            def _(b=b):
+                send_half(0, i + b)
+
+        for b in range(2):
+
+            @pl.when(i + size + b <= before)
+            def _(b=b):
+                arrive(i + size + b)
+
+        if count:
+            mixed[...] += dot(dl, lt, 0, 0)
+            rsum[...] += dot(dl, rt, 0, 1)
+        else:
+            mixed[...] = dot(dl, lt, 0, 0)
+            rsum[...] = dot(dl, rt, 0, 1)
+
+    attend(0, 0)
+    groups = (before + 1) // 2 + 1
+
+    @pl.loop(1, groups + stages)
     def _(it):
-        @pl.when(it <= before)
+        @pl.when(it < groups)
         def _():
-            attend(it)
+            attend(2 * it - 1, 2)
 
         for s in range(1, stages + 1):
-            i = it - s
-
-            @pl.when((i >= 0) & (i <= before))
-            def _():
-                half_copy(s - 1, i).wait_recv()
-                size = tok >> s
-                rows = pl.ds(pl.multiple_of(level_offset(s), size), size)
-                gpart[i, rows, :] += half_r[s - 1][i].astype(F32)
-                if s < stages:
-                    send_half(s, i)
-                else:
-
-                    @pl.when(i > 0)
-                    def _():
-                        fin_s[i] = gpart[i, rows, :].astype(BF16)
-                        fin_copy(i).start()
+            for b in range(2):
+                pass_on(s, 2 * (it - s) - 1 + b)
 
     part = o_kw.shape[0]
 
@@ -349,14 +378,14 @@
     dma = pltpu.SemaphoreType.DMA
     scratch = [pltpu.VMEM(a.shape, a.dtype) for a in args] + [
         dma((len(args),)),
-        pltpu.VMEM((span, tok, width), BF16),
-        pltpu.VMEM((span, rdim, tok), BF16),
+        pltpu.VMEM((span + 1, tok, width), BF16),
+        pltpu.VMEM((span + 1, rdim, tok), BF16),
         pltpu.VMEM((heads * tok, width), BF16),
         pltpu.VMEM((heads * tok, width), BF16),
         pltpu.VMEM((heads * tok, rpad), BF16),
         pltpu.VMEM((heads * tok, width), F32),
         pltpu.VMEM((heads * tok, rdim), F32),
-        pltpu.VMEM((span, tok, wide), F32),
+        pltpu.VMEM((span + 1, tok, wide), F32),
         pltpu.VMEM((tok, wide), F32),
         pltpu.VMEM((n_sp, part, kw.shape[1]), BF16),
         pltpu.VMEM((n_sp, part, kw.shape[1]), BF16),

time: 34.9 us -> 35.1 us (level)
  no operation moved by 1% of the time
where the time goes in v3:
time: 35.1 us; the launch traced here: 34.9 us
  Pallas kernels  34.3 us (98%)
  between operations  0.64 us (2%)
    pallas_call x1, Pallas kernels, per_device(): pl.pallas_call(functools.partial(kernel, (n_sp, n_tp, heads, factor)), ou...  33.4 us
    pallas_call x1, Pallas kernels, per_device(): pl.pallas_call(store, out_shape=[jax.ShapeDtypeStruct(s, F32) for s in sh...  0.93 us

profile of v3, /device:TPU:1, one launch (start us, length us, event | category | flops | bytes accessed | tf_op | source)
XLA Modules:
  0.0 34.9 jit_solution(1703884821625612950)
XLA Ops:
  0.6 33.4 %latent_attention_backward.1 = (f32[128,512]{1,0:T(8,128)S(1)}, f32[128,256]{1,0:T(8,128)S(1)}, f32[128,512]{1,0:T(8,128)S(1)}, f32[64,128]{1,0:T(8,128)S(1)}, f32[64,512]{1,0:T(8,128)S(1)}) custom-call(bf16[128,512]{1,0:T(8,128)(2,1)} %qm_h.1, bf16[128,256]{1,0:T(8,128)(2,1)} %qr_h.1, bf16[128,512]{1,0:T(8,128)(2,1)} %lat_h.1, bf16[64,128]{1,0:T(8,128)(2,1)} %bitcast.2, ...), custom_call_target="tpu_custom_call" | custom-call | tf_op jit(solution)/shard_map/latent_attention_backward/pallas_call | solution.py:406
  34.0 0.9 %store_outputs.1 = (f32[128,512]{1,0:T(8,128)}, f32[128,256]{1,0:T(8,128)}, f32[128,512]{1,0:T(8,128)}, f32[64,128]{1,0:T(8,128)}, f32[64,512]{1,0:T(8,128)}) custom-call(f32[128,512]{1,0:T(8,128)S(1)} %get-tuple-element.15.refs_0_, f32[128,256]{1,0:T(8,128)S(1)} %get-tuple-element.16.refs_1_, f32[128,512]{1,0:T(8,128)S(1)} %get-tuple-element.17.refs_2_, ...), custom_call_target="tpu_custom_call" | custom-call | tf_op jit(solution)/shard_map/store_outputs/pallas_call | solution.py:417

commit v4 on v3

--- a/solution.py
+++ b/solution.py
@@ -155,7 +155,7 @@
         size = tok >> (s + 1)
         bit = (tp // (1 << s)) % 2
         start = pl.multiple_of(level_offset(s) + (1 - bit) * size, size)
-        half_s[s][i] = gpart[i, pl.ds(start, size), :].astype(BF16)
+        half_s[s][i] = gpart[i, pl.ds(start, size), :].astype(half_s[s].dtype)
         half_copy(s, i).start()
 
     def fin_copy(i):
@@ -240,13 +240,13 @@
 
     @pl.loop(1, groups + stages)
     def _(it):
+        for s in range(1, stages + 1):
+            for b in range(2):
+                pass_on(s, 2 * (it - s) - 1 + b)
+
         @pl.when(it < groups)
         def _():
             attend(2 * it - 1, 2)
-
-        for s in range(1, stages + 1):
-            for b in range(2):
-                pass_on(s, 2 * (it - s) - 1 + b)
 
     part = o_kw.shape[0]
 
@@ -294,7 +294,7 @@
         ).wait_recv()
         gpart[0, my_rows, :] += fin_r[i].astype(F32)
 
-    obuf[my_rows] = gpart[0, my_rows, :]
+    obuf[my_rows] = gpart[0, my_rows, :].astype(BF16)
 
     def ag_copy(t):
         return pltpu.make_async_remote_copy(
@@ -323,8 +323,8 @@
             send_sem=agsend.at[t], recv_sem=agrecv.at[t],
             device_id={"tp": peer}, device_id_type=MESH,
         ).wait_recv()
-    o_lat[...] = obuf[:, :width]
-    o_krot[...] = obuf[:, width:].T[:rdim]
+    o_lat[...] = obuf[:, :width].astype(F32)
+    o_krot[...] = obuf[:, width:].astype(F32).T[:rdim]
 
     @pl.loop(1, after + 1)
     def _(i):
@@ -386,7 +386,7 @@
         pltpu.VMEM((heads * tok, width), F32),
         pltpu.VMEM((heads * tok, rdim), F32),
         pltpu.VMEM((span + 1, tok, wide), F32),
-        pltpu.VMEM((tok, wide), F32),
+        pltpu.VMEM((tok, wide), BF16),
         pltpu.VMEM((n_sp, part, kw.shape[1]), BF16),
         pltpu.VMEM((n_sp, part, kw.shape[1]), BF16),
         pltpu.VMEM((span, quarter, wide), BF16),
@@ -394,7 +394,9 @@
         dma((span, 2)), dma((span, 2)), dma((span, 2)), dma((span, 2)),
         dma((span,)), dma((span,)), dma((n_tp,)), dma((n_tp,)), dma((n_sp,)), dma((n_sp,)),
     ]
-    halves = [pltpu.VMEM((span, tok >> (s + 1), wide), BF16) for s in range(stages)]
+    halves = [
+        pltpu.VMEM((span, tok >> (s + 1), wide), BF16 if s else F32) for s in range(stages)
+    ]
     sems = [dma((span,)) for s in range(stages)]
     scratch = scratch + halves + halves + sems + sems
     shapes = (

time: 35.1 us -> 33.5 us (0.954)
  Pallas kernels: 34.3 us -> 32.5 us
    pallas_call x1, Pallas kernels: 33.4 us -> 31.6 us  [per_device(): pl.pallas_call(functools.partial(kernel, (n_sp, n_tp, heads, factor)), ou...]
where the time goes in v4:
time: 33.5 us; the launch traced here: 33.2 us
  Pallas kernels  32.5 us (97%)
  between operations  0.64 us (2%)
    pallas_call x1, Pallas kernels, per_device(): pl.pallas_call(functools.partial(kernel, (n_sp, n_tp, heads, factor)), ou...  31.6 us
    pallas_call x1, Pallas kernels, per_device(): pl.pallas_call(store, out_shape=[jax.ShapeDtypeStruct(s, F32) for s in sh...  0.93 us

profile of v4, /device:TPU:1, one launch (start us, length us, event | category | flops | bytes accessed | tf_op | source)
XLA Modules:
  0.0 33.2 jit_solution(17320735085189863718)
XLA Ops:
  0.6 31.6 %latent_attention_backward.1 = (f32[128,512]{1,0:T(8,128)S(1)}, f32[128,256]{1,0:T(8,128)S(1)}, f32[128,512]{1,0:T(8,128)S(1)}, f32[64,128]{1,0:T(8,128)S(1)}, f32[64,512]{1,0:T(8,128)S(1)}) custom-call(bf16[128,512]{1,0:T(8,128)(2,1)} %qm_h.1, bf16[128,256]{1,0:T(8,128)(2,1)} %qr_h.1, bf16[128,512]{1,0:T(8,128)(2,1)} %lat_h.1, bf16[64,128]{1,0:T(8,128)(2,1)} %bitcast.2, ...), custom_call_target="tpu_custom_call" | custom-call | tf_op jit(solution)/shard_map/latent_attention_backward/pallas_call | solution.py:408
  32.2 0.9 %store_outputs.1 = (f32[128,512]{1,0:T(8,128)}, f32[128,256]{1,0:T(8,128)}, f32[128,512]{1,0:T(8,128)}, f32[64,128]{1,0:T(8,128)}, f32[64,512]{1,0:T(8,128)}) custom-call(f32[128,512]{1,0:T(8,128)S(1)} %get-tuple-element.15.refs_0_, f32[128,256]{1,0:T(8,128)S(1)} %get-tuple-element.16.refs_1_, f32[128,512]{1,0:T(8,128)S(1)} %get-tuple-element.17.refs_2_, ...), custom_call_target="tpu_custom_call" | custom-call | tf_op jit(solution)/shard_map/store_outputs/pallas_call | solution.py:419
